TPU v7x, 1024 devices: a whole 4x4x32 slice. The times are simulated.
1024 devices in a mesh: rep: 32 (over z), fs: 4 (over y), tp: 8 (over x, core).
Axes of the slice: x: 4, y: 4, z: 32, core: 2. Of those that a mesh axis runs over, the one named last changes fastest.
Arguments:
- inputs: bfloat16 [20480, 2048], P('rep', 'fs'), may hold values from -6 to 6
- gate_pre: bfloat16 [20480, 5632], P('rep', 'tp'), may hold values from -12 to 12
- up_pre: bfloat16 [20480, 5632], P('rep', 'tp'), may hold values from -6 to 6
- cotangent: bfloat16 [20480, 2048], P('rep'), may hold values from -6 to 6
- w_gate: bfloat16 [2048, 5632], P('fs', 'tp'), may hold values from -0.125 to 0.125
- w_up: bfloat16 [2048, 5632], P('fs', 'tp'), may hold values from -0.125 to 0.125
- w_down: bfloat16 [5632, 2048], P('tp', 'fs'), may hold values from -0.078125 to 0.078125
Outputs:
- grad_input: bfloat16 [20480, 2048], P('rep', 'fs')
- grad_gate: float32 [64, 32, 5632], P('fs', 'rep', 'tp')
- grad_up: float32 [64, 32, 5632], P('fs', 'rep', 'tp')
- grad_down: float32 [5632, 64, 32], P('tp', 'fs', 'rep')
- gate_norms: float32 [64, 32], P('fs', 'rep')
- up_norms: float32 [64, 32], P('fs', 'rep')
- down_norms: float32 [5632], P('tp')
All inputs are finite; a program needn't handle non-finite values.
Results may differ from a plain program's by a relative error of at most 0.02.
Values may be sent and summed in bfloat16 or wider, within the bound.
A program may use at most 64 MiB of HBM per device.

v0:
```python
import functools

import jax
import jax.numpy as jnp
from jax import lax
from jax.sharding import PartitionSpec as P


def in_blocks(value, dim, devices):
    before, after = (value.shape[:dim], value.shape[dim + 1 :])
    return jnp.moveaxis(value.reshape(*before, devices, -1, *after), dim, 0)


def sent_and_summed(value, axis, dim):
    tiles = in_blocks(value, dim, lax.axis_size(axis))
    arrived = lax.all_to_all(tiles, axis, split_axis=0, concat_axis=0, tiled=True)
    return arrived.astype(jnp.float32).sum(axis=0)


def one_axis_at_a_time(value, axes):
    return functools.reduce(lax.psum, axes, value)


def on_device(inputs, gate_pre, up_pre, cotangent, w_gate, w_up, w_down):
    single = jnp.float32
    groups = lax.axis_size("rep")
    width = w_down.shape[1]
    own_cot = lax.dynamic_slice_in_dim(cotangent, lax.axis_index("fs") * width, width, 1)
    columns = cotangent
    hidden_grad = jnp.einsum(
        "td,fd->tf",
        columns,
        lax.all_gather(w_down, "fs", axis=1, tiled=True),
        preferred_element_type=single,
    )
    gate = gate_pre.astype(single)
    upper = up_pre.astype(single)
    sigma = jax.nn.sigmoid(gate)
    active = gate * sigma
    hidden = (active * upper).astype(jnp.bfloat16)
    d_up = (hidden_grad * active).astype(jnp.bfloat16)
    d_gate = (hidden_grad * upper * sigma * (1.0 + gate * (1.0 - sigma))).astype(jnp.bfloat16)
    factor = float(inputs.shape[0] * groups) ** (-0.5)
    owned = width // groups
    hunits = w_gate.shape[1]
    gate_local = jnp.einsum("td,tf->df", inputs, d_gate, preferred_element_type=single) * factor
    gate_parts = lax.all_to_all(
        gate_local.reshape(owned, groups, hunits).astype(jnp.bfloat16),
        "rep",
        split_axis=1,
        concat_axis=1,
        tiled=True,
    ).astype(jnp.float32)
    grad_gate = jnp.sum(gate_parts, axis=1, keepdims=True)
    up_local = jnp.einsum("td,tf->df", inputs, d_up, preferred_element_type=single) * factor
    up_parts = lax.all_to_all(
        up_local.reshape(owned, groups, hunits).astype(jnp.bfloat16),
        "rep",
        split_axis=1,
        concat_axis=1,
        tiled=True,
    ).astype(jnp.float32)
    grad_up = jnp.sum(up_parts, axis=1, keepdims=True)
    ordered = (
        own_cot.reshape(own_cot.shape[0], owned, groups)
        .transpose(0, 2, 1)
        .reshape(own_cot.shape[0], width)
    )
    columns = ordered
    down_owned = sent_and_summed(
        (jnp.einsum("tp,tf->pf", columns, hidden, preferred_element_type=single) * factor).astype(
            jnp.bfloat16
        ),
        "rep",
        0,
    )
    grad_down = down_owned.T.reshape(hunits, owned, 1)
    input_term = jnp.einsum("tf,df->td", d_gate, w_gate, preferred_element_type=single)
    input_term = input_term + jnp.einsum("tf,df->td", d_up, w_up, preferred_element_type=single)
    grad_input = lax.psum(input_term.astype(jnp.bfloat16), "tp")
    gate_norms, up_norms = lax.psum(
        (jnp.sum(grad_gate * grad_gate, axis=2), jnp.sum(grad_up * grad_up, axis=2)), "tp"
    )
    down_norms = one_axis_at_a_time(jnp.sum(grad_down * grad_down, axis=(1, 2)), ("rep", "fs"))
    return (grad_input, grad_gate, grad_up, grad_down, gate_norms, up_norms, down_norms)


def solution(mesh):
    placed = (
        P("rep", "fs"),
        P("rep", "tp"),
        P("rep", "tp"),
        P("rep", None),
        P("fs", "tp"),
        P("fs", "tp"),
        P("tp", "fs"),
    )
    return jax.shard_map(
        on_device,
        mesh=mesh,
        in_specs=placed,
        out_specs=(
            P("rep", "fs"),
            P("fs", "rep", "tp"),
            P("fs", "rep", "tp"),
            P("tp", "fs", "rep"),
            P("fs", "rep"),
            P("fs", "rep"),
            P("tp"),
        ),
        check_vma=False,
    )
```

profile of v0, /device:TPU:1, one launch (start us, length us, event | category | flops | bytes accessed | tf_op | source)
XLA Modules:
  0.0 385.9 jit_solution(5990271845847183739)
XLA Ops:
  7.2 1.7 copy-done
  9.0 1.1 copy.26
  10.1 1.3 copy.24
  11.3 2.2 fusion.10
  13.6 1.2 copy.25
  14.8 29.3 %all-to-all-start.2 = ((bf16[32,16,704]{2,1,0:T(8,128)(2,1)}), bf16[32,16,704]{2,1,0:T(8,128)(2,1)S(1)}, u32[]{:S(2)}, u32[]{:S(2)}) async-start(bf16[32,16,704]{2,1,0:T(8,128)(2,1)} %bitcast.28), calls=%async_computation.2 | async-start | bytes 1572864 | tf_op jit(solution)/shard_map/all_to_all | solution.py:16
  44.1 0.7 all-gather.2.cloned.1.call-update
  44.8 58.7 %all-gather.2.cloned.1.call-done = bf16[704,2048]{1,0:T(8,128)(2,1)} async-done(((bf16[704,512]{1,0:T(8,128)(2,1)}), bf16[704,2048]{1,0:T(8,128)(2,1)}) %all-gather.2.cloned.1.call-update) | async-done | bytes 2883600 | tf_op jit(solution)/shard_map/all_gather | solution.py:33
  103.5 6.2 %multiply_convert_fusion = (bf16[640,704]{0,1:T(8,128)(2,1)}, bf16[640,704]{0,1:T(8,128)(2,1)S(1)}) fusion(bf16[640,704]{0,1:T(8,128)(2,1)} %param.8, bf16[640,704]{0,1:T(8,128)(2,1)} %param.9, bf16[640,2048]{1,0:T(8,128)(2,1)S(1)} %copy-done, bf16[704,2048]{1,0:T(8,128)(2,1)} %all-gather.2.cloned.1.call-done), kind=kOutput, calls=%fused_computation.13 | convolution fusion | flops 1852252160 | bytes 9109504 | tf_op jit(solution)/shard_map/td,fd->tf/dot_general | solution.py:30
  109.6 0.9 copy-done.4
  110.6 1.6 fusion.13
  112.2 2.3 copy.19
  114.4 2.5 copy.20
  116.9 13.4 %all-to-all-done.2 = bf16[32,16,704]{2,1,0:T(8,128)(2,1)S(1)} async-done(((bf16[32,16,704]{2,1,0:T(8,128)(2,1)}), bf16[32,16,704]{2,1,0:T(8,128)(2,1)S(1)}, u32[]{:S(2)}, u32[]{:S(2)}) %all-to-all-start.2) | async-done | bytes 720928 | tf_op jit(solution)/shard_map/all_to_all | solution.py:16
  130.3 9.3 %all-to-all-start = ((bf16[16,32,704]{2,0,1:T(8,128)(2,1)}), bf16[16,32,704]{2,0,1:T(8,128)(2,1)}, u32[]{:S(2)}, u32[]{:S(2)}) async-start(bf16[16,32,704]{2,0,1:T(8,128)(2,1)} %copy.20), calls=%async_computation | async-start | bytes 1572864 | tf_op jit(solution)/shard_map/all_to_all | solution.py:47
  139.7 3.0 fusion.12
  142.6 2.3 copy.21
  144.9 2.5 copy.22
  147.3 78.4 %all-to-all-done = bf16[16,32,704]{2,0,1:T(8,128)(2,1)} async-done(((bf16[16,32,704]{2,0,1:T(8,128)(2,1)}), bf16[16,32,704]{2,0,1:T(8,128)(2,1)}, u32[]{:S(2)}, u32[]{:S(2)}) %all-to-all-start) | async-done | bytes 720928 | tf_op jit(solution)/shard_map/all_to_all | solution.py:47
  225.7 4.6 %all-to-all-start.1 = ((bf16[16,32,704]{2,0,1:T(8,128)(2,1)}), bf16[16,32,704]{2,0,1:T(8,128)(2,1)}, u32[]{:S(2)}, u32[]{:S(2)}) async-start(bf16[16,32,704]{2,0,1:T(8,128)(2,1)} %copy.22), calls=%async_computation.1 | async-start | bytes 1572864 | tf_op jit(solution)/shard_map/all_to_all | solution.py:56
  230.5 2.2 fusion.16
  232.7 1.5 fusion.11
  234.3 0.1 convert_reduce_fusion
  234.4 0.7 reshape.41
  235.1 104.6 %psum.38 = f32[704]{0:T(1024)S(1)} all-reduce(f32[704]{0:T(1024)S(1)} %multiply_reduce_fusion), channel_id=1, replica_groups=mesh['rep'=32,'fs'=4,'tp'=8] {'rep'}, use_global_device_ids=true, to_apply=%region_9.0 | all-reduce | flops 704 | bytes 5632 | tf_op jit(solution)/shard_map/psum | solution.py:21
  339.7 7.0 %psum.39 = f32[704]{0:T(1024)} all-reduce(f32[704]{0:T(1024)S(1)} %psum.38), channel_id=1, replica_groups=mesh['rep'=32,'fs'=4,'tp'=8] {'fs'}, use_global_device_ids=true, to_apply=%region_10.0 | all-reduce | flops 704 | bytes 5632 | tf_op jit(solution)/shard_map/psum | solution.py:21
  346.6 1.3 convert_reduce_fusion.2
  347.9 0.7 broadcast_in_dim.6
  348.6 1.3 convert_reduce_fusion.1
  349.8 0.7 broadcast_in_dim.7
  350.7 26.3 %all-reduce = (f32[16,1]{0,1:T(1,128)}, f32[16,1]{0,1:T(1,128)}) all-reduce(f32[16,1]{0,1:T(1,128)S(1)} %bitcast.35, f32[16,1]{0,1:T(1,128)S(1)} %bitcast.34), channel_id=1, replica_groups=mesh['rep'=32,'fs'=4,'tp'=8] {'tp'}, use_global_device_ids=true, to_apply=%region_5.0 | all-reduce | flops 32 | bytes 256 | tf_op jit(solution)/shard_map/psum | solution.py:81
  377.1 2.0 copy.28
  (17 shorter events, 0.4 us)
Async XLA Ops:
  7.2 1.7 copy-start
  14.8 115.5 %all-to-all-start.2 = ((bf16[32,16,704]{2,1,0:T(8,128)(2,1)}), bf16[32,16,704]{2,1,0:T(8,128)(2,1)S(1)}, u32[]{:S(2)}, u32[]{:S(2)}) async-start(bf16[32,16,704]{2,1,0:T(8,128)(2,1)} %bitcast.28), calls=%async_computation.2 | async-start | bytes 1572864 | tf_op jit(solution)/shard_map/all_to_all | solution.py:16
  44.0 59.4 %all-gather.2.cloned.1.call-start = ((), (), s32[]{:S(2)}) async-start(), calls=%async_computation.3 | async-start | bytes 3604480 | tf_op jit(solution)/shard_map/all_gather | solution.py:33
  103.5 7.1 %copy-start.2 = (bf16[640,512]{1,0:T(8,128)(2,1)S(1)}, bf16[640,512]{1,0:T(8,128)(2,1)}, u32[]{:S(2)}) copy-start(bf16[640,512]{1,0:T(8,128)(2,1)} %param.7) | copy-start | bytes 1966084
  109.6 0.9 copy-start.4
  130.3 95.4 %all-to-all-start = ((bf16[16,32,704]{2,0,1:T(8,128)(2,1)}), bf16[16,32,704]{2,0,1:T(8,128)(2,1)}, u32[]{:S(2)}, u32[]{:S(2)}) async-start(bf16[16,32,704]{2,0,1:T(8,128)(2,1)} %copy.20), calls=%async_computation | async-start | bytes 1572864 | tf_op jit(solution)/shard_map/all_to_all | solution.py:47
  225.7 122.8 %all-to-all-start.1 = ((bf16[16,32,704]{2,0,1:T(8,128)(2,1)}), bf16[16,32,704]{2,0,1:T(8,128)(2,1)}, u32[]{:S(2)}, u32[]{:S(2)}) async-start(bf16[16,32,704]{2,0,1:T(8,128)(2,1)} %copy.22), calls=%async_computation.1 | async-start | bytes 1572864 | tf_op jit(solution)/shard_map/all_to_all | solution.py:56
  230.4 146.7 %all-reduce.3.cloned.1.call-start = ((), (), s32[]{:S(2)}) async-start(), calls=%async_computation.4 | async-start | bytes 1310720 | tf_op jit(solution)/shard_map/psum | solution.py:80
  230.4 2.2 copy-start.1
  230.5 2.2 copy-start.3
Sparse Core Ops, SparseCore 0:
  47.5 55.8 all-gather.1
  234.4 99.1 all-reduce.2
where the time goes:
time: 387 us; the launch traced here: 386 us
  waiting for transfers between devices  151 us (39%)
  blocking collectives  138 us (36%)
  starting transfers between devices  43.3 us (11%)
  local copies, waits for them, and re-layouts  19.6 us (5%)
  matrix products  16.7 us (4%)
  between operations  14.1 us (4%)
    psum x2, blocking collectives, one_axis_at_a_time(): return functools.reduce(lax.psum, axes, value)  112 us
    all_to_all x1, waiting for transfers between devices, on_device(): lax.all_to_all(gate_local.reshape(owned, groups, hunits).astype(jnp.bfloa...  78.4 us
    all_gather x1, waiting for transfers between devices, on_device(): lax.all_gather(w_down, 'fs', axis=1, tiled=True)  58.7 us
    all_to_all x1, starting transfers between devices, sent_and_summed(): lax.all_to_all(tiles, axis, split_axis=0, concat_axis=0, tiled=True)  29.3 us
    psum x1, blocking collectives, on_device(): lax.psum((jnp.sum(grad_gate * grad_gate, axis=2), jnp.sum(grad_up * grad_...  26.3 us
    all_to_all x1, waiting for transfers between devices, sent_and_summed(): lax.all_to_all(tiles, axis, split_axis=0, concat_axis=0, tiled=True)  13.4 us
    all_to_all x1, starting transfers between devices, on_device(): lax.all_to_all(gate_local.reshape(owned, groups, hunits).astype(jnp.bfloa...  9.34 us
  transfers between devices with their start and end apart: 5, of which 3 were waited for; matrix products, arithmetic and copies ran while one was open for 7% of the time, Pallas kernels for 0%

commit v1 on v0

v1 whole, which is shorter than its diff:
```python
import functools

import jax
import jax.numpy as jnp
from jax import lax
from jax.experimental import pallas as pl
from jax.experimental.pallas import tpu as pltpu
from jax.sharding import PartitionSpec as P

MESH = pl.DeviceIdType.MESH
SINGLE = jnp.float32
HALF = jnp.bfloat16
STRIDES = (1, 1, 1, 1, 1)


def dot_nt(a, b):
    return lax.dot_general(a, b, (((1,), (1,)), ((), ())), preferred_element_type=SINGLE)


def dot_tn(a, b):
    return lax.dot_general(a, b, (((0,), (0,)), ((), ())), preferred_element_type=SINGLE)


def chains_of(groups, stride):
    half = groups // 2
    found = []
    for way, far in ((1, half), (-1, groups - 1 - half)):
        for shift in range(stride):
            start = far - shift
            found.append((way, start, stride, -(-start // stride)))
    return found


def kernel(
    sizes,
    x_ref, g_ref, u_ref, cot_ref, wg_ref, wu_ref, wd_ref,
    gi_ref, gg_ref, gu_ref, gd_ref, gn_ref, un_ref, dn_ref,
    xv, gv, uv, cv, wcat, wq, relay_a, relay_b, hgb, cg, cu, hid, xp, cp, dall,
    down, quart, stage_d, stage_q, buf_d, buf_q, fin, term, parts, res,
    nvec, nrecv, dmine, dy, dgroup, dfar,
    load_sem, a2a_s, a2a_r, hg_s, hg_r, ds_sem, dr_sem, qs_sem, qr_sem,
    ti_s, ti_r, to_s, to_r, n_s, n_r, m_s, m_r, out_sem,
):
    nr, nf, nt = sizes
    tokens, width = xv.shape
    hunits = gv.shape[0]
    q = hunits // nf
    own = width // nr
    top = -(-q // 32) * 16
    low = q - top
    rows = tokens // nt
    factor = float(tokens * nr) ** -0.5
    z, y, t = (lax.axis_index(name) for name in ("rep", "fs", "tp"))
    right, left, across = (lax.rem(y + step, nf) for step in (1, nf - 1, nf // 2))
    order = (y, left, right, across)

    def rep(step):
        return lax.rem(z + step + nr, nr)

    def at(rz=None, ry=None, rt=None):
        return (z if rz is None else rz, y if ry is None else ry, t if rt is None else rt)

    def remote(src, dst, ssem, rsem, device):
        return pltpu.make_async_remote_copy(
            src_ref=src, dst_ref=dst, send_sem=ssem, recv_sem=rsem, device_id=device, device_id_type=MESH
        )

    def arrived(ref, rsem):
        remote(ref, ref, rsem, rsem, at(ry=right)).wait_recv()

    def mult(value, by):
        return pl.multiple_of(value * by, by)

    sent = []

    def send(*args):
        copy = remote(*args)
        copy.start()
        sent.append(copy)

    loads = {}

    def load(name, src, dst):
        copy = pltpu.make_async_copy(src, dst, load_sem.at[len(loads)])
        copy.start()
        loads[name] = copy

    load("g", g_ref, gv)
    load("u", u_ref, uv)
    load("c", cot_ref, cv)
    load("x", x_ref, xv)
    load("wq", wd_ref.at[pl.ds(mult(y, q), q)], wq.at[y])
    for j in range(nf):
        load(f"wg{j}", wg_ref.at[pl.ds(j * q, q)], wcat.at[j, pl.ds(0, q)])
        load(f"wu{j}", wu_ref.at[pl.ds(j * q, q)], wcat.at[j, pl.ds(q, q)])

    barrier = pltpu.get_barrier_semaphore()
    near = [at(rz=rep(way * step)) for step in (1, 2, 3) for way in (1, -1)]
    near += [at(ry=lax.rem(y + step, nf)) for step in range(1, nf)]
    near += [at(rt=lax.rem(t + step, nt)) for step in range(1, nt)]
    for device in near:
        pl.semaphore_signal(barrier, inc=1, device_id=device, device_id_type=MESH)
    pl.semaphore_wait(barrier, len(near))

    far_a = wd_ref.at[pl.ds(pl.multiple_of(across * q, 16), top)]
    far_b = wd_ref.at[pl.ds(pl.multiple_of(across * q + top, 16), low)]
    send(far_a, relay_a, a2a_s.at[0], a2a_r.at[0], at(ry=right))
    send(far_b, relay_b, a2a_s.at[1], a2a_r.at[1], at(ry=left))
    send(wd_ref.at[pl.ds(mult(right, q), q)], wq.at[y], a2a_s.at[2], a2a_r.at[2], at(ry=right))
    send(wd_ref.at[pl.ds(mult(left, q), q)], wq.at[y], a2a_s.at[3], a2a_r.at[3], at(ry=left))

    loads["g"].wait()
    loads["u"].wait()
    step_rows = 16

    def factors(index, carry):
        span = pl.ds(pl.multiple_of(index * step_rows, step_rows), step_rows)
        gate = gv[span, :].astype(SINGLE)
        upper = uv[span, :].astype(SINGLE)
        sigma = 1.0 / (1.0 + jnp.exp(-gate))
        active = gate * sigma
        cu[span, :] = active
        hid[span, :] = (active * upper).astype(HALF)
        cg[span, :] = upper * sigma * (1.0 + gate * (1.0 - sigma))
        return carry

    lax.fori_loop(0, hunits // step_rows, factors, 0)

    place = lax.broadcasted_iota(jnp.int32, (width, width), 0)
    column = lax.broadcasted_iota(jnp.int32, (width, width), 1)
    bits = own.bit_length() - 1
    origin = (place & (own - 1)) * nr + (place >> bits)
    pick = jnp.where(column == origin, 1.0, 0.0).astype(HALF)
    loads["c"].wait()
    cp[...] = dot_nt(pick, cv[:, pl.ds(mult(y, width), width)]).astype(HALF)
    down[...] = dot_nt(cp[...], hid[...]) * factor

    specs = [chains_of(nr, stride) for stride in STRIDES]

    def tables(s):
        if s == 0:
            return down, stage_d, buf_d, ds_sem, dr_sem
        i = s - 1
        return quart.at[i], stage_q.at[i], buf_q.at[i], qs_sem.at[i], qr_sem.at[i]

    clock = [0] * len(specs)

    def local(mine, owner):
        return mine[pl.ds(mult(owner, own), own), :]

    def tick(s):
        tau = clock[s]
        clock[s] += 1
        mine, stage, buf, ssem, rsem = tables(s)
        done = []
        for c, (way, far, stride, steps) in enumerate(specs[s]):
            if tau > steps:
                continue
            distance = far - stride * tau
            if tau == 0:
                src = stage.at[c]
                src[...] = local(mine, rep(way * distance)).astype(HALF)
            else:
                src = buf.at[c, tau - 1]
                arrived(src, rsem.at[c, tau - 1])
                if tau == steps:
                    continue
                total = src[...].astype(SINGLE) + local(mine, rep(way * distance))
                src[...] = total.astype(HALF)
            send(src, buf.at[c, tau], ssem.at[c, tau], rsem.at[c, tau], at(rz=rep(way * min(stride, distance))))

    def length(s):
        return max(steps for _, _, _, steps in specs[s])

    def total_of(s):
        mine, _, buf, _, _ = tables(s)
        total = local(mine, z)
        for c, (_, _, _, steps) in enumerate(specs[s]):
            total = total + buf[c, steps - 1].astype(SINGLE)
        return total

    tick(0)

    loads["x"].wait()
    xp[...] = dot_nt(pick, xv[...]).astype(HALF)

    arrived(relay_a, a2a_r.at[0])
    send(relay_a, wq.at[left, pl.ds(0, top)], a2a_s.at[4], a2a_r.at[4], at(ry=right))
    arrived(relay_b, a2a_r.at[1])
    send(relay_b, wq.at[right, pl.ds(top, low)], a2a_s.at[5], a2a_r.at[5], at(ry=left))
    tick(0)

    def piece(j):
        return dot_nt(wq[j], cv[:, pl.ds(mult(j, width), width)])

    loads["wq"].wait()
    arrived(wq.at[left], a2a_r.at[2])
    arrived(wq.at[right], a2a_r.at[3])
    part = piece(y) + piece(left) + piece(right)
    tick(0)
    arrived(wq.at[across, pl.ds(0, top)], a2a_r.at[4])
    arrived(wq.at[across, pl.ds(top, low)], a2a_r.at[5])
    hgb[y] = (part + piece(across)).astype(HALF)
    upper_rows, lower_rows = pl.ds(0, top), pl.ds(top, low)
    send(hgb.at[y, upper_rows], hgb.at[y, upper_rows], hg_s.at[0], hg_r.at[0], at(ry=right))
    send(hgb.at[y, lower_rows], hgb.at[y, lower_rows], hg_s.at[1], hg_r.at[1], at(ry=left))
    send(hgb.at[y, lower_rows], hgb.at[y, lower_rows], hg_s.at[2], hg_r.at[2], at(ry=right))
    send(hgb.at[y, upper_rows], hgb.at[y, upper_rows], hg_s.at[3], hg_r.at[3], at(ry=left))

    def quarter(i):
        j = order[i]
        span = pl.ds(mult(j, q), q)
        grad = hgb[j].astype(SINGLE)
        dall[i, 0:q, :] = (grad * cg[span, :]).astype(HALF)
        dall[i, q : 2 * q, :] = (grad * cu[span, :]).astype(HALF)
        quart[i] = dot_nt(xp[...], dall[i]) * factor
        tick(1 + i)

    quarter(0)
    tick(0)
    tick(1)
    arrived(hgb.at[left, upper_rows], hg_r.at[0])
    send(hgb.at[left, upper_rows], hgb.at[left, upper_rows], hg_s.at[4], hg_r.at[4], at(ry=right))
    arrived(hgb.at[right, lower_rows], hg_r.at[1])
    send(hgb.at[right, lower_rows], hgb.at[right, lower_rows], hg_s.at[5], hg_r.at[5], at(ry=left))
    tick(0)
    tick(1)
    arrived(hgb.at[left, lower_rows], hg_r.at[2])
    quarter(1)
    arrived(hgb.at[right, upper_rows], hg_r.at[3])
    quarter(2)
    tick(0)
    tick(1)
    arrived(hgb.at[across, upper_rows], hg_r.at[4])
    arrived(hgb.at[across, lower_rows], hg_r.at[5])
    quarter(3)

    for name in [f"w{kind}{j}" for kind in "gu" for j in range(nf)]:
        loads[name].wait()

    block = 128

    def terms(n):
        span = pl.ds(n * block, block)
        total = dot_tn(dall[0, :, span], wcat[order[0]])
        for i in range(1, nf):
            total = total + dot_tn(dall[i, :, span], wcat[order[i]])
        term[span, :] = total.astype(HALF)

    peers = [lax.rem(t + step, nt) for step in range(1, nt)]

    def terms_out():
        for n, peer in enumerate(peers):
            send(term.at[pl.ds(mult(peer, rows), rows)], parts.at[t], ti_s.at[n], ti_r.at[n], at(rt=peer))
        parts[t] = term[pl.ds(mult(t, rows), rows), :]

    def sources():
        return [lax.rem(t + nt - step, nt) for step in range(1, nt)]

    def terms_sum():
        for n, peer in enumerate(sources()):
            arrived(parts.at[peer], ti_r.at[n])
        total = parts[0].astype(SINGLE)
        for n in range(1, nt):
            total = total + parts[n].astype(SINGLE)
        res[...] = total.astype(HALF)
        for n, peer in enumerate(peers):
            send(res, gi_ref.at[t], to_s.at[n], to_r.at[n], at(rt=peer))
        pltpu.make_async_copy(res, gi_ref.at[t], out_sem).start()

    def terms_end():
        for n, peer in enumerate(sources()):
            arrived(gi_ref.at[peer], to_r.at[n])
        pltpu.make_async_copy(res, gi_ref.at[t], out_sem).wait()

    def exchange(slots, mine, count, base, device_of):
        slots[mine] = dmine[...]
        for step in range(1, count):
            n = base + step - 1
            send(dmine, slots.at[mine], m_s.at[n], m_r.at[n], device_of(lax.rem(mine + step, count)))

    def summed(slots, mine, count, base):
        for step in range(1, count):
            arrived(slots.at[lax.rem(mine + count - step, count)], m_r.at[base + step - 1])
        total = slots[0]
        for n in range(1, count):
            total = total + slots[n]
        return total

    group = 4
    inner, outer = lax.rem(z, group), z // group
    across_y = (dy, y, nf, 0)
    across_in = (dgroup, inner, group, nf - 1)
    across_out = (dfar, outer, nr // group, nf + group - 2)
    dscr = (dmine,)

    def down_first():
        total = total_of(0)
        gd_ref[...] = total
        dmine[...] = jnp.sum(total * total, axis=0, keepdims=True)
        exchange(*across_y, lambda p: at(ry=p))

    def down_second():
        nvalue = summed(*across_y)
        dgroup[inner] = nvalue
        for step in range(1, group):
            n = nf - 1 + step - 1
            peer = lax.rem(inner + step, group)
            send(dgroup.at[inner], dgroup.at[inner], m_s.at[n], m_r.at[n], at(rz=outer * group + peer))

    def down_third():
        dfar[outer] = summed(*across_in)
        count = nr // group
        for step in range(1, count):
            n = nf + group - 2 + step - 1
            peer = lax.rem(outer + step, count)
            send(dfar.at[outer], dfar.at[outer], m_s.at[n], m_r.at[n], at(rz=peer * group + inner))

    def down_last():
        dn_ref[...] = summed(*across_out)

    down_stage = [down_first, down_second, down_third]

    n_tick = 0
    while clock[4] <= length(4):
        n_tick += 1
        for s in (4, 3, 2, 1, 0):
            if clock[s] <= length(s):
                tick(s)
        if 1 <= n_tick <= tokens // block:
            terms(n_tick - 1)
            if n_tick == tokens // block:
                terms_out()
        if n_tick == tokens // block + 5:
            terms_sum()
        if clock[0] > length(0) and down_stage:
            down_stage.pop(0)()
    while down_stage:
        down_stage.pop(0)()

    for i in range(nf):
        fin[order[i]] = total_of(1 + i)
    gate_total = jnp.zeros((own, 1), SINGLE)
    up_total = jnp.zeros((own, 1), SINGLE)
    for j in range(nf):
        gate_part, up_part = fin[j, :, 0:q], fin[j, :, q : 2 * q]
        gg_ref[:, j * q : (j + 1) * q] = gate_part
        gu_ref[:, j * q : (j + 1) * q] = up_part
        gate_total = gate_total + jnp.sum(gate_part * gate_part, axis=1, keepdims=True)
        up_total = up_total + jnp.sum(up_part * up_part, axis=1, keepdims=True)
    lane = lax.broadcasted_iota(jnp.int32, (own, 128), 1)
    nvec[...] = jnp.where(lane < 64, gate_total, up_total)
    nrecv[t] = nvec[...]
    for n, peer in enumerate(peers):
        send(nvec, nrecv.at[t], n_s.at[n], n_r.at[n], at(rt=peer))
    terms_end()
    for n, peer in enumerate(sources()):
        arrived(nrecv.at[peer], n_r.at[n])
    norms = nrecv[0]
    for n in range(1, nt):
        norms = norms + nrecv[n]
    turned = norms.T
    gn_ref[...] = turned[0:1, :]
    un_ref[...] = turned[64:65, :]
    down_last()
    for copy in sent:
        copy.wait_send()


def on_device(inputs, gate_pre, up_pre, cotangent, w_gate, w_up, w_down):
    nr, nf, nt = (lax.axis_size(name) for name in ("rep", "fs", "tp"))
    tokens, width = inputs.shape
    hunits = w_gate.shape[1]
    q, own, rows = hunits // nf, width // nr, tokens // nt
    top = -(-q // 32) * 16
    features = cotangent.shape[1]
    chain_count = [2 * stride for stride in STRIDES]
    many = max(chain_count[1:])
    long_d = -(-(nr // 2) // STRIDES[0])
    long_q = max(-(-(nr // 2) // stride) for stride in STRIDES[1:])
    vmem, dma = pltpu.VMEM, pltpu.SemaphoreType.DMA
    any_space = pl.BlockSpec(memory_space=pl.ANY)
    in_vmem = pl.BlockSpec(memory_space=pltpu.VMEM)
    shape = jax.ShapeDtypeStruct
    small = (nf - 1) + 3 + (nr // 4 - 1)
    gi, gg, gu, gd, gn, un, dn = pl.pallas_call(
        functools.partial(kernel, (nr, nf, nt)),
        out_shape=(
            shape((nt, rows, width), HALF),
            shape((own, hunits), SINGLE),
            shape((own, hunits), SINGLE),
            shape((own, hunits), SINGLE),
            shape((1, own), SINGLE),
            shape((1, own), SINGLE),
            shape((1, hunits), SINGLE),
        ),
        in_specs=[any_space] * 7,
        out_specs=(any_space,) + (in_vmem,) * 6,
        scratch_shapes=[
            vmem((tokens, width), HALF),
            vmem((hunits, tokens), HALF),
            vmem((hunits, tokens), HALF),
            vmem((tokens, features), HALF),
            vmem((nf, 2 * q, width), HALF),
            vmem((nf, q, width), HALF),
            vmem((top, width), HALF),
            vmem((q - top, width), HALF),
            vmem((nf, q, tokens), HALF),
            vmem((hunits, tokens), SINGLE),
            vmem((hunits, tokens), SINGLE),
            vmem((hunits, tokens), HALF),
            vmem((width, tokens), HALF),
            vmem((width, tokens), HALF),
            vmem((nf, 2 * q, tokens), HALF),
            vmem((width, hunits), SINGLE),
            vmem((nf, width, 2 * q), SINGLE),
            vmem((chain_count[0], own, hunits), HALF),
            vmem((nf, many, own, 2 * q), HALF),
            vmem((chain_count[0], long_d, own, hunits), HALF),
            vmem((nf, many, long_q, own, 2 * q), HALF),
            vmem((nf, own, 2 * q), SINGLE),
            vmem((tokens, width), HALF),
            vmem((nt, rows, width), HALF),
            vmem((rows, width), HALF),
            vmem((own, 128), SINGLE),
            vmem((nt, own, 128), SINGLE),
            vmem((1, hunits), SINGLE),
            vmem((nf, 1, hunits), SINGLE),
            vmem((4, 1, hunits), SINGLE),
            vmem((nr // 4, 1, hunits), SINGLE),
            dma((5 + 2 * nf,)),
            dma((6,)),
            dma((6,)),
            dma((6,)),
            dma((6,)),
            dma((chain_count[0], long_d)),
            dma((chain_count[0], long_d)),
            dma((nf, many, long_q)),
            dma((nf, many, long_q)),
            dma((nt - 1,)),
            dma((nt - 1,)),
            dma((nt - 1,)),
            dma((nt - 1,)),
            dma((nt - 1,)),
            dma((nt - 1,)),
            dma((small,)),
            dma((small,)),
            dma(()),
        ],
        compiler_params=pltpu.CompilerParams(
            collective_id=0, has_side_effects=True, vmem_limit_bytes=56 * 2**20
        ),
    )(inputs, gate_pre.T, up_pre.T, cotangent, w_gate.T, w_up.T, w_down)
    return (
        gi.reshape(tokens, width),
        gg.reshape(own, 1, hunits),
        gu.reshape(own, 1, hunits),
        gd.T.reshape(hunits, own, 1),
        gn.reshape(own, 1),
        un.reshape(own, 1),
        dn.reshape(hunits),
    )


def solution(mesh):
    placed = (
        P("rep", "fs"),
        P("rep", "tp"),
        P("rep", "tp"),
        P("rep", None),
        P("fs", "tp"),
        P("fs", "tp"),
        P("tp", "fs"),
    )
    return jax.shard_map(
        on_device,
        mesh=mesh,
        in_specs=placed,
        out_specs=(
            P("rep", "fs"),
            P("fs", "rep", "tp"),
            P("fs", "rep", "tp"),
            P("tp", "fs", "rep"),
            P("fs", "rep"),
            P("fs", "rep"),
            P("tp"),
        ),
        check_vma=False,
    )
```

time: 387 us -> 115 us (0.30)
  waiting for transfers between devices: 151 us -> 0 us
  blocking collectives: 138 us -> 0 us
  Pallas kernels: 0 us -> 104 us
  starting transfers between devices: 43.3 us -> 0 us
  matrix products: 16.7 us -> 0 us
  between operations: 14.1 us -> 0.65 us
  local copies, waits for them, and re-layouts: 19.6 us -> 8.68 us
    psum x3 -> x0, blocking collectives: 138 us -> none  [the longest x2 112 us: one_axis_at_a_time(): return functools.reduce(lax.psum, axes, value)]
    pallas_call x0 -> x1, Pallas kernels: none -> 104 us  [on_device(): pl.pallas_call(functools.partial(kernel, (nr, nf, nt)), out_shape=(shape(...]
    all_to_all x3 -> x0, waiting for transfers between devices: 91.8 us -> none  [the longest x1 78.4 us: on_device(): lax.all_to_all(gate_local.reshape(owned, groups, hunits).astype(jnp.bfloa...]
    all_gather x1 -> x0, waiting for transfers between devices: 58.7 us -> none  [on_device(): lax.all_gather(w_down, 'fs', axis=1, tiled=True)]
    all_to_all x3 -> x0, starting transfers between devices: 43.2 us -> none  [the longest x1 29.3 us: sent_and_summed(): lax.all_to_all(tiles, axis, split_axis=0, concat_axis=0, tiled=True)]
    dot_general x6 -> x0, matrix products: 16.7 us -> none  [the longest x1 6.16 us: on_device(): jnp.einsum('td,fd->tf', columns, lax.all_gather(w_down, 'fs', axis=1, til...]
    convert_element_type x5 -> x0, local copies, waits for them, and re-layouts: 10.6 us -> none  [the longest x2 4.73 us: on_device(): gate_local.reshape(owned, groups, hunits).astype(jnp.bfloat16)]
    unnamed x12 -> x6, local copies, waits for them, and re-layouts: 5.72 us -> 8.68 us
  transfers between devices with their start and end apart: 5 -> 0, of which waited for: 3 -> 0; matrix products, arithmetic and copies ran while one was open for 7% -> 0% of each run, Pallas kernels for 0% -> 0%
where the time goes in v1:
time: 115 us; the launch traced here: 114 us
  Pallas kernels  104 us (90%)
  local copies, waits for them, and re-layouts  8.68 us (8%)
  other arithmetic  1.28 us (1%)
    pallas_call x1, Pallas kernels, on_device(): pl.pallas_call(functools.partial(kernel, (nr, nf, nt)), out_shape=(shape(...  104 us
    unnamed x6, local copies, waits for them, and re-layouts  8.68 us

profile of v1, /device:TPU:1, one launch (start us, length us, event | category | flops | bytes accessed | tf_op | source)
XLA Modules:
  0.0 114.3 jit_solution(7627318578445789781)
XLA Ops:
  0.6 103.7 %shard_map.126 = (bf16[8,80,512]{2,1,0:T(8,128)(2,1)}, f32[16,704]{1,0:T(8,128)}, f32[16,704]{1,0:T(8,128)}, f32[16,704]{1,0:T(8,128)}, f32[1,16]{1,0:T(1,128)}, /*index=5*/f32[1,16]{1,0:T(1,128)}, f32[1,704]{1,0:T(1,128)}) custom-call(bf16[640,512]{1,0:T(8,128)(2,1)} %x_ref.1, bf16[704,640]{1,0:T(8,128)(2,1)} %bitcast.12, bf16[704,640]{1,0:T(8,128)(2,1)} %bitcast.13, ...), custom_call_target="tpu_custom_call" | custom-call | tf_op jit(solution)/shard_map/pallas_call | solution.py:386
  104.3 1.5 %copy.14 = f32[16,1,704]{2,1,0:T(1,128)} copy(f32[16,1,704]{2,0,1:T(8,128)} %bitcast.19) | data formatting | bytes 90112
  105.8 1.3 %reduce = f32[704]{0:T(1024)} reduce(f32[1,704]{1,0:T(1,128)} %get-tuple-element.20, f32[]{:T(128)} %constant), dimensions={0}, to_apply=%get-tuple-element.20.reduce_sub_computation | reduce | bytes 5636 | tf_op jit(solution)/shard_map/pallas_call | solution.py:386
  107.0 1.5 %copy.15 = f32[16,1,704]{2,1,0:T(1,128)} copy(f32[16,1,704]{2,0,1:T(8,128)} %bitcast.18) | data formatting | bytes 90112
  108.5 1.5 %copy.16 = f32[704,16,1]{0,2,1:T(1,128)} copy(f32[704,16,1]{0,1,2:T(8,128)} %bitcast.17) | data formatting | bytes 90112
  110.0 2.0 %copy.20 = bf16[640,512]{1,0:T(8,128)(2,1)} copy(bf16[640,512]{1,0:T(8,128)(2,1)} %bitcast.16) | data formatting | bytes 1310720
  111.9 1.1 copy.21
  113.1 1.2 %copy.22 = f32[16,1]{0,1:T(1,128)} copy(f32[16,1]{0,1:T(1,128)} %bitcast.20) | data formatting | bytes 128

commit v2 on v1

--- a/solution.py
+++ b/solution.py
@@ -10,7 +10,10 @@
 MESH = pl.DeviceIdType.MESH
 SINGLE = jnp.float32
 HALF = jnp.bfloat16
-STRIDES = (1, 1, 1, 1, 1)
+STRIDES = (2, 2, 2, 2, 2)
+PER_TICK = 2
+WAITS = 5
+ROUND = (1, 0, 2, 3, 4)
 
 
 def dot_nt(a, b):
@@ -25,10 +28,13 @@
     half = groups // 2
     found = []
     for way, far in ((1, half), (-1, groups - 1 - half)):
-        for shift in range(stride):
-            start = far - shift
-            found.append((way, start, stride, -(-start // stride)))
+        links = far // stride
+        found.append((way, far, links, 0 if links * stride == far else 1))
     return found
+
+
+def side_count(groups, stride):
+    return (groups // 2 - 1) // stride + 1
 
 
 def kernel(
@@ -36,10 +42,10 @@
     x_ref, g_ref, u_ref, cot_ref, wg_ref, wu_ref, wd_ref,
     gi_ref, gg_ref, gu_ref, gd_ref, gn_ref, un_ref, dn_ref,
     xv, gv, uv, cv, wcat, wq, relay_a, relay_b, hgb, cg, cu, hid, xp, cp, dall,
-    down, quart, stage_d, stage_q, buf_d, buf_q, fin, term, parts, res,
+    fin, term, parts, res,
     nvec, nrecv, dmine, dy, dgroup, dfar,
-    load_sem, a2a_s, a2a_r, hg_s, hg_r, ds_sem, dr_sem, qs_sem, qr_sem,
-    ti_s, ti_r, to_s, to_r, n_s, n_r, m_s, m_r, out_sem,
+    load_sem, a2a_s, a2a_r, hg_s, hg_r,
+    ti_s, ti_r, to_s, to_r, n_s, n_r, m_s, m_r, out_sem, *chain_refs,
 ):
     nr, nf, nt = sizes
     tokens, width = xv.shape
@@ -95,7 +101,7 @@
         load(f"wu{j}", wu_ref.at[pl.ds(j * q, q)], wcat.at[j, pl.ds(q, q)])
 
     barrier = pltpu.get_barrier_semaphore()
-    near = [at(rz=rep(way * step)) for step in (1, 2, 3) for way in (1, -1)]
+    near = [at(rz=rep(way * step)) for step in range(1, max(3, *STRIDES) + 1) for way in (1, -1)]
     near += [at(ry=lax.rem(y + step, nf)) for step in range(1, nf)]
     near += [at(rt=lax.rem(t + step, nt)) for step in range(1, nt)]
     for device in near:
@@ -133,50 +139,84 @@
     pick = jnp.where(column == origin, 1.0, 0.0).astype(HALF)
     loads["c"].wait()
     cp[...] = dot_nt(pick, cv[:, pl.ds(mult(y, width), width)]).astype(HALF)
-    down[...] = dot_nt(cp[...], hid[...]) * factor
+    sets = [chain_refs[9 * n : 9 * n + 9] for n in range(len(STRIDES))]
+    sets[0][0][...] = dot_nt(cp[...], hid[...]) * factor
 
     specs = [chains_of(nr, stride) for stride in STRIDES]
-
-    def tables(s):
-        if s == 0:
-            return down, stage_d, buf_d, ds_sem, dr_sem
-        i = s - 1
-        return quart.at[i], stage_q.at[i], buf_q.at[i], qs_sem.at[i], qr_sem.at[i]
-
     clock = [0] * len(specs)
 
     def local(mine, owner):
         return mine[pl.ds(mult(owner, own), own), :]
 
     def tick(s):
+        with jax.named_scope(f"tick#s={s}"):
+            step(s)
+
+    def sides(s, c, piece):
+        _, _, _, side_src, side_dst, _, _, side_s, side_r = sets[s]
+        count = side_count(nr, STRIDES[s])
+        span = pl.ds(count // 2, count - count // 2) if piece == 0 else pl.ds(0, count // 2)
+        for r in range(1, STRIDES[s]):
+            yield r, side_src.at[c, r - 1, span], side_dst.at[c, r - 1, span], side_s.at[c, r - 1, piece], side_r.at[c, r - 1, piece]
+
+    def launch_sides(s):
+        mine, _, _, side_src, _, _, _, _, _ = sets[s]
+        stride = STRIDES[s]
+        count = side_count(nr, stride)
+        for piece in (0, 1):
+            for c, (way, far, _, _) in enumerate(specs[s]):
+                for r in range(1, stride):
+                    for m in range(count // 2, count) if piece == 0 else range(count // 2):
+                        side_src[c, r - 1, m] = local(mine, rep(way * (stride * m + r))).astype(HALF)
+            for c, (way, _, _, _) in enumerate(specs[s]):
+                for r, src, dst, ssem, rsem in sides(s, c, piece):
+                    send(src, dst, ssem, rsem, at(rz=rep(way * r)))
+
+    def step(s):
         tau = clock[s]
         clock[s] += 1
-        mine, stage, buf, ssem, rsem = tables(s)
-        done = []
-        for c, (way, far, stride, steps) in enumerate(specs[s]):
-            if tau > steps:
+        mine, stage, buf, _, side_dst, ssem, rsem, _, _ = sets[s]
+        stride = STRIDES[s]
+        count = side_count(nr, stride)
+        for c, (way, far, links, delay) in enumerate(specs[s]):
+            k = tau - delay
+            m = links - k
+            if tau == 1:
+                for _, _, dst, _, rsem_side in sides(s, c, 0):
+                    arrived(dst, rsem_side)
+            if m == count // 2 - 1:
+                for _, _, dst, _, rsem_side in sides(s, c, 1):
+                    arrived(dst, rsem_side)
+            if not 0 <= k <= links:
                 continue
-            distance = far - stride * tau
-            if tau == 0:
+            if k > 0:
+                arrived(buf.at[c, k - 1], rsem.at[c, k - 1])
+            if k == links:
+                continue
+            total = local(mine, rep(way * stride * m))
+            for r in range(1, stride):
+                if stride * m + r <= far:
+                    total = total + side_dst[c, r - 1, m].astype(SINGLE)
+            if k == 0:
                 src = stage.at[c]
-                src[...] = local(mine, rep(way * distance)).astype(HALF)
             else:
-                src = buf.at[c, tau - 1]
-                arrived(src, rsem.at[c, tau - 1])
-                if tau == steps:
-                    continue
-                total = src[...].astype(SINGLE) + local(mine, rep(way * distance))
-                src[...] = total.astype(HALF)
-            send(src, buf.at[c, tau], ssem.at[c, tau], rsem.at[c, tau], at(rz=rep(way * min(stride, distance))))
+                src = buf.at[c, k - 1]
+                total = total + src[...].astype(SINGLE)
+            src[...] = total.astype(HALF)
+            send(src, buf.at[c, k], ssem.at[c, k], rsem.at[c, k], at(rz=rep(way * stride)))
+        if tau == 0:
+            launch_sides(s)
 
     def length(s):
-        return max(steps for _, _, _, steps in specs[s])
+        return max(links + delay for _, _, links, delay in specs[s])
 
     def total_of(s):
-        mine, _, buf, _, _ = tables(s)
+        mine, _, buf, _, side_dst, _, _, _, _ = sets[s]
         total = local(mine, z)
-        for c, (_, _, _, steps) in enumerate(specs[s]):
-            total = total + buf[c, steps - 1].astype(SINGLE)
+        for c, (_, _, links, _) in enumerate(specs[s]):
+            total = total + buf[c, links - 1].astype(SINGLE)
+            for r in range(1, STRIDES[s]):
+                total = total + side_dst[c, r - 1, 0].astype(SINGLE)
         return total
 
     tick(0)
@@ -197,7 +237,6 @@
     arrived(wq.at[left], a2a_r.at[2])
     arrived(wq.at[right], a2a_r.at[3])
     part = piece(y) + piece(left) + piece(right)
-    tick(0)
     arrived(wq.at[across, pl.ds(0, top)], a2a_r.at[4])
     arrived(wq.at[across, pl.ds(top, low)], a2a_r.at[5])
     hgb[y] = (part + piece(across)).astype(HALF)
@@ -213,12 +252,11 @@
         grad = hgb[j].astype(SINGLE)
         dall[i, 0:q, :] = (grad * cg[span, :]).astype(HALF)
         dall[i, q : 2 * q, :] = (grad * cu[span, :]).astype(HALF)
-        quart[i] = dot_nt(xp[...], dall[i]) * factor
+        sets[1 + i][0][...] = dot_nt(xp[...], dall[i]) * factor
         tick(1 + i)
 
     quarter(0)
     tick(0)
-    tick(1)
     arrived(hgb.at[left, upper_rows], hg_r.at[0])
     send(hgb.at[left, upper_rows], hgb.at[left, upper_rows], hg_s.at[4], hg_r.at[4], at(ry=right))
     arrived(hgb.at[right, lower_rows], hg_r.at[1])
@@ -319,24 +357,23 @@
     def down_last():
         dn_ref[...] = summed(*across_out)
 
+    blocks = tokens // block
+    input_stage = [functools.partial(terms, n) for n in range(blocks)]
+    input_stage += [terms_out] + [lambda: None] * WAITS + [terms_sum]
     down_stage = [down_first, down_second, down_third]
-
     n_tick = 0
-    while clock[4] <= length(4):
+    while any(clock[s] <= length(s) for s in ROUND):
         n_tick += 1
-        for s in (4, 3, 2, 1, 0):
+        for s in ROUND:
             if clock[s] <= length(s):
                 tick(s)
-        if 1 <= n_tick <= tokens // block:
-            terms(n_tick - 1)
-            if n_tick == tokens // block:
-                terms_out()
-        if n_tick == tokens // block + 5:
-            terms_sum()
+        for _ in range(PER_TICK):
+            if input_stage:
+                input_stage.pop(0)()
         if clock[0] > length(0) and down_stage:
             down_stage.pop(0)()
-    while down_stage:
-        down_stage.pop(0)()
+    for stage in input_stage + down_stage:
+        stage()
 
     for i in range(nf):
         fin[order[i]] = total_of(1 + i)
@@ -367,6 +404,16 @@
         copy.wait_send()
 
 
+def finish(gi_ref, gg_ref, gu_ref, gd_ref, gn_ref, un_ref, dn_ref, *out):
+    gi_out, gg_out, gu_out, gd_out, gn_out, un_out, dn_out = out
+    gi_out[...] = gi_ref[...]
+    for src, dst in ((gg_ref, gg_out), (gu_ref, gu_out), (gd_ref, gd_out)):
+        dst[...] = src[...].reshape(dst.shape)
+    gn_out[...] = gn_ref[...]
+    un_out[...] = un_ref[...]
+    dn_out[...] = dn_ref[0, :]
+
+
 def on_device(inputs, gate_pre, up_pre, cotangent, w_gate, w_up, w_down):
     nr, nf, nt = (lax.axis_size(name) for name in ("rep", "fs", "tp"))
     tokens, width = inputs.shape
@@ -374,14 +421,25 @@
     q, own, rows = hunits // nf, width // nr, tokens // nt
     top = -(-q // 32) * 16
     features = cotangent.shape[1]
-    chain_count = [2 * stride for stride in STRIDES]
-    many = max(chain_count[1:])
-    long_d = -(-(nr // 2) // STRIDES[0])
-    long_q = max(-(-(nr // 2) // stride) for stride in STRIDES[1:])
     vmem, dma = pltpu.VMEM, pltpu.SemaphoreType.DMA
     any_space = pl.BlockSpec(memory_space=pl.ANY)
     in_vmem = pl.BlockSpec(memory_space=pltpu.VMEM)
     shape = jax.ShapeDtypeStruct
+    chain_scratch = []
+    for stride, lanes in zip(STRIDES, (hunits,) + (2 * q,) * nf):
+        links = nr // 2 // stride
+        side = (2, max(stride - 1, 1), side_count(nr, stride))
+        chain_scratch += [
+            vmem((width, lanes), SINGLE),
+            vmem((2, own, lanes), HALF),
+            vmem((2, links, own, lanes), HALF),
+            vmem((*side, own, lanes), HALF),
+            vmem((*side, own, lanes), HALF),
+            dma((2, links)),
+            dma((2, links)),
+            dma((2, side[1], 2)),
+            dma((2, side[1], 2)),
+        ]
     small = (nf - 1) + 3 + (nr // 4 - 1)
     gi, gg, gu, gd, gn, un, dn = pl.pallas_call(
         functools.partial(kernel, (nr, nf, nt)),
@@ -412,12 +470,6 @@
             vmem((width, tokens), HALF),
             vmem((width, tokens), HALF),
             vmem((nf, 2 * q, tokens), HALF),
-            vmem((width, hunits), SINGLE),
-            vmem((nf, width, 2 * q), SINGLE),
-            vmem((chain_count[0], own, hunits), HALF),
-            vmem((nf, many, own, 2 * q), HALF),
-            vmem((chain_count[0], long_d, own, hunits), HALF),
-            vmem((nf, many, long_q, own, 2 * q), HALF),
             vmem((nf, own, 2 * q), SINGLE),
             vmem((tokens, width), HALF),
             vmem((nt, rows, width), HALF),
@@ -433,10 +485,6 @@
             dma((6,)),
             dma((6,)),
             dma((6,)),
-            dma((chain_count[0], long_d)),
-            dma((chain_count[0], long_d)),
-            dma((nf, many, long_q)),
-            dma((nf, many, long_q)),
             dma((nt - 1,)),
             dma((nt - 1,)),
             dma((nt - 1,)),
@@ -446,19 +494,34 @@
             dma((small,)),
             dma((small,)),
             dma(()),
+            *chain_scratch,
         ],
         compiler_params=pltpu.CompilerParams(
             collective_id=0, has_side_effects=True, vmem_limit_bytes=56 * 2**20
         ),
     )(inputs, gate_pre.T, up_pre.T, cotangent, w_gate.T, w_up.T, w_down)
+    gi, gg, gu, gd, gn, un, dn = pl.pallas_call(
+        finish,
+        out_shape=(
+            shape((nt, rows, width), HALF),
+            shape((own, 1, hunits), SINGLE),
+            shape((own, 1, hunits), SINGLE),
+            shape((own, 1, hunits), SINGLE),
+            shape((1, own), SINGLE),
+            shape((1, own), SINGLE),
+            shape((hunits,), SINGLE),
+        ),
+        in_specs=[in_vmem] * 7,
+        out_specs=(in_vmem,) * 7,
+    )(gi, gg, gu, gd, gn, un, dn)
     return (
         gi.reshape(tokens, width),
-        gg.reshape(own, 1, hunits),
-        gu.reshape(own, 1, hunits),
-        gd.T.reshape(hunits, own, 1),
+        gg,
+        gu,
+        gd.transpose(2, 0, 1),
         gn.reshape(own, 1),
         un.reshape(own, 1),
-        dn.reshape(hunits),
+        dn,
     )
 
 

time: 115 us -> 92.1 us (0.80)
  Pallas kernels: 104 us -> 90.6 us
  local copies, waits for them, and re-layouts: 8.68 us -> 0 us
  other arithmetic: 1.28 us -> 0 us
    pallas_call x1, Pallas kernels: 104 us -> 88.6 us  [on_device(): pl.pallas_call(functools.partial(kernel, (nr, nf, nt)), out_shape=(shape(...]
    unnamed x6 -> x0, local copies, waits for them, and re-layouts: 8.68 us -> none
    pallas_call x0 -> x1, Pallas kernels: none -> 2.07 us  [on_device(): pl.pallas_call(finish, out_shape=(shape((nt, rows, width), HALF), shape((...]
    pallas_call x1 -> x0, other arithmetic: 1.28 us -> none  [on_device(): pl.pallas_call(functools.partial(kernel, (nr, nf, nt)), out_shape=(shape(...]
where the time goes in v2:
time: 92.1 us; the launch traced here: 91.3 us
  Pallas kernels  90.6 us (98%)
    pallas_call x1, Pallas kernels, on_device(): pl.pallas_call(functools.partial(kernel, (nr, nf, nt)), out_shape=(shape(...  88.6 us
    pallas_call x1, Pallas kernels, on_device(): pl.pallas_call(finish, out_shape=(shape((nt, rows, width), HALF), shape((...  2.07 us

profile of v2, /device:TPU:1, one launch (start us, length us, event | category | flops | bytes accessed | tf_op | source)
XLA Modules:
  0.0 91.3 jit_solution(8845662998471891947)
XLA Ops:
  0.6 88.6 %shard_map.126 = (bf16[8,80,512]{2,1,0:T(8,128)(2,1)}, f32[16,704]{1,0:T(8,128)}, f32[16,704]{1,0:T(8,128)}, f32[16,704]{1,0:T(8,128)}, f32[1,16]{1,0:T(1,128)}, /*index=5*/f32[1,16]{1,0:T(1,128)}, f32[1,704]{1,0:T(1,128)}) custom-call(bf16[640,512]{1,0:T(8,128)(2,1)} %x_ref.1, bf16[704,640]{1,0:T(8,128)(2,1)} %bitcast.8, bf16[704,640]{1,0:T(8,128)(2,1)} %bitcast.9, ...), custom_call_target="tpu_custom_call" | custom-call | tf_op jit(solution)/shard_map/pallas_call | solution.py:444
  89.2 2.1 %shard_map.127 = (bf16[8,80,512]{2,1,0:T(8,128)(2,1)}, f32[16,1,704]{2,1,0:T(1,128)}, f32[16,1,704]{2,1,0:T(1,128)}, f32[16,1,704]{2,1,0:T(1,128)}, f32[1,16]{1,...) custom-call(bf16[8,80,512]{2,1,0:T(8,128)(2,1)} %get-tuple-element.21.gi_ref, f32[16,704]{1,0:T(8,128)} %get-tuple-element.22.gg_ref, ...), custom_call_target="tpu_custom_call" | custom-call | tf_op jit(solution)/shard_map/pallas_call | solution.py:503

commit v3 on v2

--- a/solution.py
+++ b/solution.py
@@ -13,7 +13,9 @@
 STRIDES = (2, 2, 2, 2, 2)
 PER_TICK = 2
 WAITS = 5
-ROUND = (1, 0, 2, 3, 4)
+ROUND = (1, 2, 3, 4, 0)
+PIECE = (2, 4, 1, 1, 1)
+LEAD = (4, 8, 1, 1, 1)
 
 
 def dot_nt(a, b):
@@ -41,11 +43,11 @@
     sizes,
     x_ref, g_ref, u_ref, cot_ref, wg_ref, wu_ref, wd_ref,
     gi_ref, gg_ref, gu_ref, gd_ref, gn_ref, un_ref, dn_ref,
-    xv, gv, uv, cv, wcat, wq, relay_a, relay_b, hgb, cg, cu, hid, xp, cp, dall,
+    xv, gv, uv, cv, wv, wcat, wq, relay_a, relay_b, hgb, cg, cu, hid, xp, cp, dall,
     fin, term, parts, res,
-    nvec, nrecv, dmine, dy, dgroup, dfar,
+    nvec, nrecv, dnear, dfar,
     load_sem, a2a_s, a2a_r, hg_s, hg_r,
-    ti_s, ti_r, to_s, to_r, n_s, n_r, m_s, m_r, out_sem, *chain_refs,
+    ti_s, ti_r, to_s, to_r, n_s, n_r, m_s, m_r, f_s, f_r, out_sem, *chain_refs,
 ):
     nr, nf, nt = sizes
     tokens, width = xv.shape
@@ -91,6 +93,7 @@
         copy.start()
         loads[name] = copy
 
+    load("w", wd_ref, wv)
     load("g", g_ref, gv)
     load("u", u_ref, uv)
     load("c", cot_ref, cv)
@@ -101,20 +104,11 @@
         load(f"wu{j}", wu_ref.at[pl.ds(j * q, q)], wcat.at[j, pl.ds(q, q)])
 
     barrier = pltpu.get_barrier_semaphore()
-    near = [at(rz=rep(way * step)) for step in range(1, max(3, *STRIDES) + 1) for way in (1, -1)]
+    near = [at(rz=rep(way * step)) for step in range(1, max(2, *STRIDES) + 1) for way in (1, -1)]
     near += [at(ry=lax.rem(y + step, nf)) for step in range(1, nf)]
     near += [at(rt=lax.rem(t + step, nt)) for step in range(1, nt)]
     for device in near:
         pl.semaphore_signal(barrier, inc=1, device_id=device, device_id_type=MESH)
-    pl.semaphore_wait(barrier, len(near))
-
-    far_a = wd_ref.at[pl.ds(pl.multiple_of(across * q, 16), top)]
-    far_b = wd_ref.at[pl.ds(pl.multiple_of(across * q + top, 16), low)]
-    send(far_a, relay_a, a2a_s.at[0], a2a_r.at[0], at(ry=right))
-    send(far_b, relay_b, a2a_s.at[1], a2a_r.at[1], at(ry=left))
-    send(wd_ref.at[pl.ds(mult(right, q), q)], wq.at[y], a2a_s.at[2], a2a_r.at[2], at(ry=right))
-    send(wd_ref.at[pl.ds(mult(left, q), q)], wq.at[y], a2a_s.at[3], a2a_r.at[3], at(ry=left))
-
     loads["g"].wait()
     loads["u"].wait()
     step_rows = 16
@@ -132,6 +126,16 @@
 
     lax.fori_loop(0, hunits // step_rows, factors, 0)
 
+    pl.semaphore_wait(barrier, len(near))
+
+    loads["w"].wait()
+    far_a = wv.at[pl.ds(pl.multiple_of(across * q, 16), top)]
+    far_b = wv.at[pl.ds(pl.multiple_of(across * q + top, 16), low)]
+    send(far_a, relay_a, a2a_s.at[0], a2a_r.at[0], at(ry=right))
+    send(far_b, relay_b, a2a_s.at[1], a2a_r.at[1], at(ry=left))
+    send(wv.at[pl.ds(mult(right, q), q)], wq.at[y], a2a_s.at[2], a2a_r.at[2], at(ry=right))
+    send(wv.at[pl.ds(mult(left, q), q)], wq.at[y], a2a_s.at[3], a2a_r.at[3], at(ry=left))
+
     place = lax.broadcasted_iota(jnp.int32, (width, width), 0)
     column = lax.broadcasted_iota(jnp.int32, (width, width), 1)
     bits = own.bit_length() - 1
@@ -152,40 +156,46 @@
         with jax.named_scope(f"tick#s={s}"):
             step(s)
 
+    def side_span(s, piece):
+        count, size = side_count(nr, STRIDES[s]), PIECE[s]
+        return range(count - size * (piece + 1), count - size * piece)
+
     def sides(s, c, piece):
         _, _, _, side_src, side_dst, _, _, side_s, side_r = sets[s]
-        count = side_count(nr, STRIDES[s])
-        span = pl.ds(count // 2, count - count // 2) if piece == 0 else pl.ds(0, count // 2)
+        span = pl.ds(side_span(s, piece).start, PIECE[s])
         for r in range(1, STRIDES[s]):
             yield r, side_src.at[c, r - 1, span], side_dst.at[c, r - 1, span], side_s.at[c, r - 1, piece], side_r.at[c, r - 1, piece]
 
-    def launch_sides(s):
+    def launch_sides(s, piece):
         mine, _, _, side_src, _, _, _, _, _ = sets[s]
         stride = STRIDES[s]
-        count = side_count(nr, stride)
-        for piece in (0, 1):
-            for c, (way, far, _, _) in enumerate(specs[s]):
-                for r in range(1, stride):
-                    for m in range(count // 2, count) if piece == 0 else range(count // 2):
-                        side_src[c, r - 1, m] = local(mine, rep(way * (stride * m + r))).astype(HALF)
-            for c, (way, _, _, _) in enumerate(specs[s]):
-                for r, src, dst, ssem, rsem in sides(s, c, piece):
-                    send(src, dst, ssem, rsem, at(rz=rep(way * r)))
+        for c, (way, _, _, _) in enumerate(specs[s]):
+            for r in range(1, stride):
+                for m in side_span(s, piece):
+                    side_src[c, r - 1, m] = local(mine, rep(way * (stride * m + r))).astype(HALF)
+        for c, (way, _, _, _) in enumerate(specs[s]):
+            for r, src, dst, ssem, rsem in sides(s, c, piece):
+                send(src, dst, ssem, rsem, at(rz=rep(way * r)))
+
+    def launch_due(s, tau):
+        if STRIDES[s] > 1:
+            for piece in range(side_count(nr, STRIDES[s]) // PIECE[s]):
+                if tau == max(0, 1 + PIECE[s] * piece - LEAD[s]):
+                    launch_sides(s, piece)
 
     def step(s):
         tau = clock[s]
         clock[s] += 1
         mine, stage, buf, _, side_dst, ssem, rsem, _, _ = sets[s]
         stride = STRIDES[s]
-        count = side_count(nr, stride)
+        count, size = side_count(nr, stride), PIECE[s]
+        if tau > 0:
+            launch_due(s, tau)
         for c, (way, far, links, delay) in enumerate(specs[s]):
             k = tau - delay
             m = links - k
-            if tau == 1:
-                for _, _, dst, _, rsem_side in sides(s, c, 0):
-                    arrived(dst, rsem_side)
-            if m == count // 2 - 1:
-                for _, _, dst, _, rsem_side in sides(s, c, 1):
+            if stride > 1 and tau % size == 1 % size and 1 <= tau <= count:
+                for _, _, dst, _, rsem_side in sides(s, c, (tau - 1) // size):
                     arrived(dst, rsem_side)
             if not 0 <= k <= links:
                 continue
@@ -205,7 +215,7 @@
             src[...] = total.astype(HALF)
             send(src, buf.at[c, k], ssem.at[c, k], rsem.at[c, k], at(rz=rep(way * stride)))
         if tau == 0:
-            launch_sides(s)
+            launch_due(s, tau)
 
     def length(s):
         return max(links + delay for _, _, links, delay in specs[s])
@@ -267,11 +277,10 @@
     quarter(1)
     arrived(hgb.at[right, upper_rows], hg_r.at[3])
     quarter(2)
-    tick(0)
-    tick(1)
     arrived(hgb.at[across, upper_rows], hg_r.at[4])
     arrived(hgb.at[across, lower_rows], hg_r.at[5])
     quarter(3)
+    tick(0)
 
     for name in [f"w{kind}{j}" for kind in "gu" for j in range(nf)]:
         loads[name].wait()
@@ -311,56 +320,44 @@
             arrived(gi_ref.at[peer], to_r.at[n])
         pltpu.make_async_copy(res, gi_ref.at[t], out_sem).wait()
 
-    def exchange(slots, mine, count, base, device_of):
-        slots[mine] = dmine[...]
-        for step in range(1, count):
-            n = base + step - 1
-            send(dmine, slots.at[mine], m_s.at[n], m_r.at[n], device_of(lax.rem(mine + step, count)))
-
-    def summed(slots, mine, count, base):
-        for step in range(1, count):
-            arrived(slots.at[lax.rem(mine + count - step, count)], m_r.at[base + step - 1])
-        total = slots[0]
-        for n in range(1, count):
-            total = total + slots[n]
-        return total
-
     group = 4
     inner, outer = lax.rem(z, group), z // group
-    across_y = (dy, y, nf, 0)
-    across_in = (dgroup, inner, group, nf - 1)
-    across_out = (dfar, outer, nr // group, nf + group - 2)
-    dscr = (dmine,)
+    count = nr // group
 
     def down_first():
         total = total_of(0)
         gd_ref[...] = total
-        dmine[...] = jnp.sum(total * total, axis=0, keepdims=True)
-        exchange(*across_y, lambda p: at(ry=p))
+        dnear[inner, y] = jnp.sum(total * total, axis=0, keepdims=True)
+        for n in range(1, group * nf):
+            by_z, by_y = n // nf, n % nf
+            device = at(rz=outer * group + lax.rem(inner + by_z, group), ry=lax.rem(y + by_y, nf))
+            send(dnear.at[inner, y], dnear.at[inner, y], m_s.at[n - 1], m_r.at[n - 1], device)
 
     def down_second():
-        nvalue = summed(*across_y)
-        dgroup[inner] = nvalue
-        for step in range(1, group):
-            n = nf - 1 + step - 1
-            peer = lax.rem(inner + step, group)
-            send(dgroup.at[inner], dgroup.at[inner], m_s.at[n], m_r.at[n], at(rz=outer * group + peer))
-
-    def down_third():
-        dfar[outer] = summed(*across_in)
-        count = nr // group
-        for step in range(1, count):
-            n = nf + group - 2 + step - 1
-            peer = lax.rem(outer + step, count)
-            send(dfar.at[outer], dfar.at[outer], m_s.at[n], m_r.at[n], at(rz=peer * group + inner))
+        for n in range(1, group * nf):
+            by_z, by_y = n // nf, n % nf
+            place = dnear.at[lax.rem(inner + group - by_z, group), lax.rem(y + nf - by_y, nf)]
+            arrived(place, m_r.at[n - 1])
+        total = dnear[0, 0]
+        for n in range(1, group * nf):
+            total = total + dnear[n // nf, n % nf]
+        dfar[outer] = total
+        for n in range(1, count):
+            device = at(rz=lax.rem(outer + n, count) * group + inner)
+            send(dfar.at[outer], dfar.at[outer], f_s.at[n - 1], f_r.at[n - 1], device)
 
     def down_last():
-        dn_ref[...] = summed(*across_out)
+        for n in range(1, count):
+            arrived(dfar.at[lax.rem(outer + count - n, count)], f_r.at[n - 1])
+        total = dfar[0]
+        for n in range(1, count):
+            total = total + dfar[n]
+        dn_ref[...] = total
 
     blocks = tokens // block
     input_stage = [functools.partial(terms, n) for n in range(blocks)]
     input_stage += [terms_out] + [lambda: None] * WAITS + [terms_sum]
-    down_stage = [down_first, down_second, down_third]
+    down_stage = [down_first, down_second]
     n_tick = 0
     while any(clock[s] <= length(s) for s in ROUND):
         n_tick += 1
@@ -426,7 +423,7 @@
     in_vmem = pl.BlockSpec(memory_space=pltpu.VMEM)
     shape = jax.ShapeDtypeStruct
     chain_scratch = []
-    for stride, lanes in zip(STRIDES, (hunits,) + (2 * q,) * nf):
+    for stride, size, lanes in zip(STRIDES, PIECE, (hunits,) + (2 * q,) * nf):
         links = nr // 2 // stride
         side = (2, max(stride - 1, 1), side_count(nr, stride))
         chain_scratch += [
@@ -437,10 +434,9 @@
             vmem((*side, own, lanes), HALF),
             dma((2, links)),
             dma((2, links)),
-            dma((2, side[1], 2)),
-            dma((2, side[1], 2)),
+            dma((2, side[1], side[2] // size)),
+            dma((2, side[1], side[2] // size)),
         ]
-    small = (nf - 1) + 3 + (nr // 4 - 1)
     gi, gg, gu, gd, gn, un, dn = pl.pallas_call(
         functools.partial(kernel, (nr, nf, nt)),
         out_shape=(
@@ -459,6 +455,7 @@
             vmem((hunits, tokens), HALF),
             vmem((hunits, tokens), HALF),
             vmem((tokens, features), HALF),
+            vmem((hunits, width), HALF),
             vmem((nf, 2 * q, width), HALF),
             vmem((nf, q, width), HALF),
             vmem((top, width), HALF),
@@ -476,11 +473,9 @@
             vmem((rows, width), HALF),
             vmem((own, 128), SINGLE),
             vmem((nt, own, 128), SINGLE),
-            vmem((1, hunits), SINGLE),
-            vmem((nf, 1, hunits), SINGLE),
-            vmem((4, 1, hunits), SINGLE),
+            vmem((4, nf, 1, hunits), SINGLE),
             vmem((nr // 4, 1, hunits), SINGLE),
-            dma((5 + 2 * nf,)),
+            dma((6 + 2 * nf,)),
             dma((6,)),
             dma((6,)),
             dma((6,)),
@@ -491,8 +486,10 @@
             dma((nt - 1,)),
             dma((nt - 1,)),
             dma((nt - 1,)),
-            dma((small,)),
-            dma((small,)),
+            dma((4 * nf - 1,)),
+            dma((4 * nf - 1,)),
+            dma((nr // 4 - 1,)),
+            dma((nr // 4 - 1,)),
             dma(()),
             *chain_scratch,
         ],

time: 92.1 us -> 88.3 us (0.959)
  Pallas kernels: 90.6 us -> 87.5 us
    pallas_call x1, Pallas kernels: 88.6 us -> 85.4 us  [on_device(): pl.pallas_call(functools.partial(kernel, (nr, nf, nt)), out_shape=(shape(...]
where the time goes in v3:
time: 88.3 us; the launch traced here: 88.2 us
  Pallas kernels  87.5 us (99%)
    pallas_call x1, Pallas kernels, on_device(): pl.pallas_call(functools.partial(kernel, (nr, nf, nt)), out_shape=(shape(...  85.4 us
    pallas_call x1, Pallas kernels, on_device(): pl.pallas_call(finish, out_shape=(shape((nt, rows, width), HALF), shape((...  2.07 us

profile of v3, /device:TPU:1, one launch (start us, length us, event | category | flops | bytes accessed | tf_op | source)
XLA Modules:
  0.0 88.2 jit_solution(12998000953291278244)
XLA Ops:
  0.6 85.4 %shard_map.126 = (bf16[8,80,512]{2,1,0:T(8,128)(2,1)}, f32[16,704]{1,0:T(8,128)}, f32[16,704]{1,0:T(8,128)}, f32[16,704]{1,0:T(8,128)}, f32[1,16]{1,0:T(1,128)}, /*index=5*/f32[1,16]{1,0:T(1,128)}, f32[1,704]{1,0:T(1,128)}) custom-call(bf16[640,512]{1,0:T(8,128)(2,1)} %x_ref.1, bf16[704,640]{1,0:T(8,128)(2,1)} %bitcast.8, bf16[704,640]{1,0:T(8,128)(2,1)} %bitcast.9, ...), custom_call_target="tpu_custom_call" | custom-call | tf_op jit(solution)/shard_map/pallas_call | solution.py:440
  86.1 2.1 %shard_map.127 = (bf16[8,80,512]{2,1,0:T(8,128)(2,1)}, f32[16,1,704]{2,1,0:T(1,128)}, f32[16,1,704]{2,1,0:T(1,128)}, f32[16,1,704]{2,1,0:T(1,128)}, f32[1,16]{1,...) custom-call(bf16[8,80,512]{2,1,0:T(8,128)(2,1)} %get-tuple-element.21.gi_ref, f32[16,704]{1,0:T(8,128)} %get-tuple-element.22.gg_ref, ...), custom_call_target="tpu_custom_call" | custom-call | tf_op jit(solution)/shard_map/pallas_call | solution.py:500

commit v4 on v3

--- a/solution.py
+++ b/solution.py
@@ -14,8 +14,8 @@
 PER_TICK = 2
 WAITS = 5
 ROUND = (1, 2, 3, 4, 0)
-PIECE = (2, 4, 1, 1, 1)
-LEAD = (4, 8, 1, 1, 1)
+PIECE = (2, 2, 1, 1, 1)
+LEAD = (4, 3, 1, 1, 1)
 
 
 def dot_nt(a, b):
@@ -265,8 +265,8 @@
         sets[1 + i][0][...] = dot_nt(xp[...], dall[i]) * factor
         tick(1 + i)
 
+    tick(0)
     quarter(0)
-    tick(0)
     arrived(hgb.at[left, upper_rows], hg_r.at[0])
     send(hgb.at[left, upper_rows], hgb.at[left, upper_rows], hg_s.at[4], hg_r.at[4], at(ry=right))
     arrived(hgb.at[right, lower_rows], hg_r.at[1])

time: 88.3 us -> 88.6 us (level)
  no operation moved by 1% of the time
where the time goes in v4:
time: 88.6 us; the launch traced here: 88.5 us
  Pallas kernels  87.8 us (99%)
    pallas_call x1, Pallas kernels, on_device(): pl.pallas_call(functools.partial(kernel, (nr, nf, nt)), out_shape=(shape(...  85.7 us
    pallas_call x1, Pallas kernels, on_device(): pl.pallas_call(finish, out_shape=(shape((nt, rows, width), HALF), shape((...  2.07 us

profile of v4, /device:TPU:1, one launch (start us, length us, event | category | flops | bytes accessed | tf_op | source)
XLA Modules:
  0.0 88.5 jit_solution(13937087705119143008)
XLA Ops:
  0.6 85.7 %shard_map.126 = (bf16[8,80,512]{2,1,0:T(8,128)(2,1)}, f32[16,704]{1,0:T(8,128)}, f32[16,704]{1,0:T(8,128)}, f32[16,704]{1,0:T(8,128)}, f32[1,16]{1,0:T(1,128)}, /*index=5*/f32[1,16]{1,0:T(1,128)}, f32[1,704]{1,0:T(1,128)}) custom-call(bf16[640,512]{1,0:T(8,128)(2,1)} %x_ref.1, bf16[704,640]{1,0:T(8,128)(2,1)} %bitcast.8, bf16[704,640]{1,0:T(8,128)(2,1)} %bitcast.9, ...), custom_call_target="tpu_custom_call" | custom-call | tf_op jit(solution)/shard_map/pallas_call | solution.py:440
  86.4 2.1 %shard_map.127 = (bf16[8,80,512]{2,1,0:T(8,128)(2,1)}, f32[16,1,704]{2,1,0:T(1,128)}, f32[16,1,704]{2,1,0:T(1,128)}, f32[16,1,704]{2,1,0:T(1,128)}, f32[1,16]{1,...) custom-call(bf16[8,80,512]{2,1,0:T(8,128)(2,1)} %get-tuple-element.21.gi_ref, f32[16,704]{1,0:T(8,128)} %get-tuple-element.22.gg_ref, ...), custom_call_target="tpu_custom_call" | custom-call | tf_op jit(solution)/shard_map/pallas_call | solution.py:500
